TPU v7x, 32 devices: a whole 2x2x4 slice. The times are simulated.
32 devices in a mesh: fs: 4 (over y, x), tp: 8 (over z, core).
Axes of the slice: x: 2, y: 2, z: 4, core: 2. Of those that a mesh axis runs over, the one named last changes fastest.
Arguments:
- tokens: bfloat16 [4096, 2048], P(('fs', 'tp')), may hold values from -6 to 6
- gate_weight: bfloat16 [2048, 5632], P('fs', 'tp'), may hold values from -0.125 to 0.125
- up_weight: bfloat16 [2048, 5632], P('fs', 'tp'), may hold values from -0.125 to 0.125
- down_weight: bfloat16 [5632, 2048], P('tp', 'fs'), may hold values from -0.078125 to 0.078125
- grad_out: bfloat16 [4096, 2048], P(('fs', 'tp')), may hold values from -6 to 6
Outputs:
- grad_input: bfloat16 [4096, 2048], P(('fs', 'tp'))
- grad_gate: float32 [2048, 5632], P('fs', 'tp')
- grad_up: float32 [2048, 5632], P('fs', 'tp')
- grad_down: float32 [5632, 2048], P('tp', 'fs')
All inputs are finite; a program needn't handle non-finite values.
Results may differ from a plain program's by a relative error of at most 0.0049.
Values may be sent and summed in bfloat16 or wider, within the bound.
A program may use at most 128 MiB of HBM per device.

v0:
```python
import jax
import jax.numpy as jnp
from jax import lax
from jax.sharding import PartitionSpec as P


def over_rows(left, right):
    return lax.dot_general(
        left, right, (((0,), (0,)), ((), ())), preferred_element_type=jnp.float32
    )


def over_cols(left, right):
    return lax.dot_general(
        left, right, (((1,), (1,)), ((), ())), preferred_element_type=jnp.float32
    )


def body(tokens, gate_weight, up_weight, down_weight, grad_out):
    tok_all, cot_all = (
        lax.all_gather(tokens, "tp", axis=0, tiled=True),
        lax.all_gather(grad_out, "tp", axis=0, tiled=True),
    )
    gate_full, up_full = (
        lax.all_gather(gate_weight, "fs", axis=0, tiled=True),
        lax.all_gather(up_weight, "fs", axis=0, tiled=True),
    )
    down_full = lax.all_gather(down_weight, "fs", axis=1, tiled=True)
    gate_pre = jnp.dot(tok_all, gate_full, preferred_element_type=jnp.float32)
    up_pre = jnp.dot(tok_all, up_full, preferred_element_type=jnp.float32)
    sig_gate = jax.nn.sigmoid(gate_pre)
    active = gate_pre * sig_gate
    hidden = (active * up_pre).astype(jnp.bfloat16)
    d_hidden = over_cols(cot_all, down_full)
    d_gate = (d_hidden * up_pre * sig_gate * (1.0 + gate_pre * (1.0 - sig_gate))).astype(
        jnp.bfloat16
    )
    d_up = (d_hidden * active).astype(jnp.bfloat16)
    grad_input = lax.psum_scatter(
        over_cols(d_gate, gate_full) + over_cols(d_up, up_full),
        "tp",
        scatter_dimension=0,
        tiled=True,
    ).astype(jnp.bfloat16)
    width = gate_full.shape[1]
    summed = lax.psum_scatter(
        jnp.concatenate(
            [over_rows(tok_all, d_gate), over_rows(tok_all, d_up), over_rows(cot_all, hidden)],
            axis=1,
        ),
        "fs",
        scatter_dimension=0,
        tiled=True,
    )
    grad_gate = summed[:, :width]
    grad_up = summed[:, width : 2 * width]
    grad_down = summed[:, 2 * width :].T
    return (grad_input, grad_gate, grad_up, grad_down)


def solution(mesh):
    in_specs = (
        P(("fs", "tp"), None),
        P("fs", "tp"),
        P("fs", "tp"),
        P("tp", "fs"),
        P(("fs", "tp"), None),
    )
    out_specs = (P(("fs", "tp"), None), P("fs", "tp"), P("fs", "tp"), P("tp", "fs"))
    return jax.shard_map(body, mesh=mesh, in_specs=in_specs, out_specs=out_specs, check_vma=False)
```

profile of v0, /device:TPU:0, one launch (start us, length us, event | category | flops | bytes accessed | tf_op | source)
XLA Modules:
  0.0 514.1 jit_solution(16898894607041836768)
XLA Ops:
  7.2 0.7 all-gather.12.cloned.1.call-update
  7.9 0.7 all-gather.10.cloned.1.call-update
  8.7 0.7 all-gather.14.cloned.1.call-update
  10.0 0.5 all-gather.6.cloned.1.call-update
  10.6 43.5 %all-gather.12.cloned.1.call-done = bf16[2048,704]{0,1:T(8,128)(2,1)} async-done(((bf16[512,704]{0,1:T(8,128)(2,1)}), bf16[2048,704]{0,1:T(8,128)(2,1)}) %all-gather.12.cloned.1.call-update) | async-done | bytes 2883600 | tf_op jit(solution)/shard_map/all_gather | solution.py:26
  54.1 48.5 %all-gather.10.cloned.1.call-done = bf16[1024,2048]{1,0:T(8,128)(2,1)} async-done(((bf16[128,2048]{1,0:T(8,128)(2,1)}), bf16[1024,2048]{1,0:T(8,128)(2,1)}) %all-gather.10.cloned.1.call-update) | async-done | bytes 4194320 | tf_op jit(solution)/shard_map/all_gather | solution.py:21
  102.6 7.8 %fusion.3 = f32[1024,704]{0,1:T(8,128)} fusion(bf16[1024,2048]{1,0:T(8,128)(2,1)} %all-gather.10.cloned.1.call-done, bf16[2048,704]{0,1:T(8,128)(2,1)} %all-gather.12.cloned.1.call-done), kind=kOutput, calls=%fused_computation.12 | convolution fusion | flops 2952790016 | bytes 9961472 | tf_op jit(solution)/shard_map/dot_general | solution.py:30
  110.4 34.4 %all-gather.14.cloned.1.call-done = bf16[2048,704]{0,1:T(8,128)(2,1)} async-done(((bf16[512,704]{0,1:T(8,128)(2,1)}), bf16[2048,704]{0,1:T(8,128)(2,1)}) %all-gather.14.cloned.1.call-update) | async-done | bytes 2883600 | tf_op jit(solution)/shard_map/all_gather | solution.py:25
  144.8 7.9 %fusion.4 = f32[1024,704]{0,1:T(8,128)} fusion(bf16[1024,2048]{1,0:T(8,128)(2,1)} %all-gather.10.cloned.1.call-done, bf16[2048,704]{0,1:T(8,128)(2,1)} %all-gather.14.cloned.1.call-done), kind=kOutput, calls=%fused_computation.13 | convolution fusion | flops 2952790016 | bytes 9961472 | tf_op jit(solution)/shard_map/dot_general | solution.py:29
  152.7 35.3 %all-gather.8.cloned.1.call-done = bf16[704,2048]{1,0:T(8,128)(2,1)} async-done(((bf16[704,512]{1,0:T(8,128)(2,1)}), bf16[704,2048]{1,0:T(8,128)(2,1)}) %all-gather.8.cloned.1.call-update) | async-done | bytes 2883600 | tf_op jit(solution)/shard_map/all_gather | solution.py:28
  188.1 48.3 %all-gather.6.cloned.1.call-done = bf16[1024,2048]{1,0:T(8,128)(2,1)} async-done(((bf16[128,2048]{1,0:T(8,128)(2,1)}), bf16[1024,2048]{1,0:T(8,128)(2,1)}) %all-gather.6.cloned.1.call-update) | async-done | bytes 4194320 | tf_op jit(solution)/shard_map/all_gather | solution.py:22
  236.4 8.6 %multiply_convert_fusion.1 = (bf16[1024,704]{0,1:T(8,128)(2,1)S(1)}, bf16[1024,704]{0,1:T(8,128)(2,1)S(1)}) fusion(f32[1024,704]{0,1:T(8,128)} %fusion.4, f32[1024,704]{0,1:T(8,128)} %fusion.3, bf16[1024,2048]{1,0:T(8,128)(2,1)} %all-gather.6.cloned.1.call-done, bf16[704,2048]{1,0:T(8,128)(2,1)} %all-gather.8.cloned.1.call-done), kind=kOutput, calls=%fused_computation.6 | convolution fusion | flops 2962161664 | bytes 15728640 | tf_op jit(solution)/shard_map/dot_general | solution.py:14
  245.1 3.5 fusion.5
  248.6 6.1 %convolution_add_fusion = f32[1024,2048]{1,0:T(8,128)} fusion(f32[1024,2048]{1,0:T(8,128)S(1)} %fusion.5, bf16[1024,704]{0,1:T(8,128)(2,1)S(1)} %get-tuple-element.4, bf16[2048,704]{0,1:T(8,128)(2,1)S(1)} %copy-done.2), kind=kOutput, calls=%fused_computation.1 | convolution fusion | flops 2954887168 | bytes 21102592 | tf_op jit(solution)/shard_map/dot_general | solution.py:14
  254.8 1.3 copy-done.5
  256.1 5.1 convolution_bitcast_fusion.1
  261.2 3.2 convolution_bitcast_fusion.2
  264.4 0.7 copy-done.9
  265.1 3.2 convolution_bitcast_fusion
  268.3 6.5 %pad_maximum_fusion = f32[2048,2112]{0,1:T(8,128)} fusion(f32[2048,704]{0,1:T(8,128)S(1)} %convolution_bitcast_fusion, f32[2048,704]{0,1:T(8,128)S(1)} %convolution_bitcast_fusion.1, f32[2048,704]{0,1:T(8,128)S(1)} %convolution_bitcast_fusion.2), kind=kLoop, calls=%fused_computation | loop fusion | flops 8650752 | bytes 34603008 | tf_op jit(solution)/shard_map/concatenate | solution.py:47
  274.9 68.4 %reduce-scatter.3.cloned.1.call-done = f32[128,2048]{1,0:T(8,128)} async-done(((f32[1024,2048]{1,0:T(8,128)}), f32[128,2048]{1,0:T(8,128)}) %reduce-scatter.3.cloned.1.call-update) | async-done | bytes 1048592 | tf_op jit(solution)/shard_map/reduce_scatter | solution.py:39
  343.2 2.1 convert_element_type.14
  345.3 157.5 %reduce-scatter.5.cloned.1.call-done = f32[512,2112]{0,1:T(8,128)} async-done(((f32[2048,2112]{0,1:T(8,128)}), f32[512,2112]{0,1:T(8,128)}) %reduce-scatter.5.cloned.1.call-update) | async-done | bytes 4325392 | tf_op jit(solution)/shard_map/reduce_scatter | solution.py:46
  502.8 4.4 slice_bitcast_fusion
  (28 shorter events, 0.9 us)
Async XLA Ops:
  7.2 46.9 %all-gather.12.cloned.1.call-start = ((), (), s32[]{:S(2)}) async-start(), calls=%async_computation.5 | async-start | bytes 3604480 | tf_op jit(solution)/shard_map/all_gather | solution.py:26
  7.9 94.7 %all-gather.10.cloned.1.call-start = ((), (), s32[]{:S(2)}) async-start(), calls=%async_computation.4 | async-start | bytes 4718592 | tf_op jit(solution)/shard_map/all_gather | solution.py:21
  8.6 136.2 %all-gather.14.cloned.1.call-start = ((), (), s32[]{:S(2)}) async-start(), calls=%async_computation.6 | async-start | bytes 3604480 | tf_op jit(solution)/shard_map/all_gather | solution.py:25
  9.4 178.7 %all-gather.8.cloned.1.call-start = ((), (), s32[]{:S(2)}) async-start(), calls=%async_computation.3 | async-start | bytes 3604480 | tf_op jit(solution)/shard_map/all_gather | solution.py:28
  10.0 226.4 %all-gather.6.cloned.1.call-start = ((), (), s32[]{:S(2)}) async-start(), calls=%async_computation.2 | async-start | bytes 4718592 | tf_op jit(solution)/shard_map/all_gather | solution.py:22
  10.5 332.7 %reduce-scatter.3.cloned.1.call-start = ((), (), s32[]{:S(2)}) async-start(), calls=%async_computation.7 | async-start | bytes 9437184 | tf_op jit(solution)/shard_map/reduce_scatter | solution.py:39
  152.7 92.3 %copy-start.3 = (bf16[2048,704]{0,1:T(8,128)(2,1)S(1)}, bf16[2048,704]{0,1:T(8,128)(2,1)}, u32[]{:S(2)}) copy-start(bf16[2048,704]{0,1:T(8,128)(2,1)} %all-gather.14.cloned.1.call-done) | copy-start | bytes 8650756
  245.0 3.6 copy-start.6
  245.0 3.6 copy-start.4
  245.1 3.6 copy-start.2
  254.7 1.4 copy-start.5
  254.7 6.4 %copy-start.7 = (bf16[1024,704]{0,1:T(8,128)(2,1)S(1)}, bf16[1024,704]{0,1:T(8,128)(2,1)}, u32[]{:S(2)}) copy-start(bf16[1024,704]{0,1:T(8,128)(2,1)} %copy-done.6) | copy-start | bytes 4325380
  254.8 248.1 %reduce-scatter.5.cloned.1.call-start = ((), (), s32[]{:S(2)}) async-start(), calls=%async_computation.8 | async-start | bytes 21626880 | tf_op jit(solution)/shard_map/reduce_scatter | solution.py:46
  256.1 5.1 copy-start
  261.2 3.2 copy-start.1
  261.2 3.2 copy-start.8
  261.2 3.9 copy-start.9
Sparse Core Ops, SparseCore 0:
  9.8 44.2 all-gather.11
  55.7 46.8 all-gather.9
  104.4 40.3 all-gather.13
  146.5 41.5 all-gather.7
  189.5 46.8 all-gather.5
  254.9 88.3 reduce-scatter.2
  346.4 156.4 reduce-scatter.4
where the time goes:
time: 514 us
  waiting for transfers between devices  439 us (85%)
  matrix products  45.4 us (9%)
  between operations  14.3 us (3%)
  other arithmetic  8.6 us (2%)
  local copies, waits for them, and re-layouts  6.37 us (1%)
    reduce_scatter x1, waiting for transfers between devices, body(): lax.psum_scatter(jnp.concatenate([over_rows(tok_all, d_gate), over_rows(t...  158 us
    reduce_scatter x1, waiting for transfers between devices, body(): lax.psum_scatter(over_cols(d_gate, gate_full) + over_cols(d_up, up_full),...  68.4 us
    all_gather x1, waiting for transfers between devices, body(): lax.all_gather(tokens, 'tp', axis=0, tiled=True)  48.5 us
    all_gather x1, waiting for transfers between devices, body(): lax.all_gather(grad_out, 'tp', axis=0, tiled=True)  48.3 us
    all_gather x1, waiting for transfers between devices, body(): lax.all_gather(up_weight, 'fs', axis=0, tiled=True)  43.5 us
    all_gather x1, waiting for transfers between devices, body(): down_full = lax.all_gather(down_weight, 'fs', axis=1, tiled=True)  35.3 us
    all_gather x1, waiting for transfers between devices, body(): lax.all_gather(gate_weight, 'fs', axis=0, tiled=True)  34.4 us
    dot_general x3, matrix products, over_cols(): lax.dot_general(left, right, (((1,), (1,)), ((), ())), preferred_element_...  18.2 us
  transfers between devices with their start and end apart: 7, of which 7 were waited for; matrix products, arithmetic and copies ran while one was open for 7% of the time, Pallas kernels for 0%

commit v1 on v0

--- a/solution.py
+++ b/solution.py
@@ -17,10 +17,14 @@
 
 
 def body(tokens, gate_weight, up_weight, down_weight, grad_out):
-    tok_all, cot_all = (
-        lax.all_gather(tokens, "tp", axis=0, tiled=True),
-        lax.all_gather(grad_out, "tp", axis=0, tiled=True),
-    )
+
+    def lay_the_things(s0):
+        arr_out = lax.axis_size("tp")
+        z1 = jnp.stack([s0] * arr_out)
+        part_now = lax.all_to_all(z1, "tp", 0, 0)
+        return jnp.concatenate(part_now, axis=0)
+
+    tok_all, cot_all = (lay_the_things(tokens), lax.all_gather(grad_out, "tp", axis=0, tiled=True))
     gate_full, up_full = (
         lax.all_gather(gate_weight, "fs", axis=0, tiled=True),
         lax.all_gather(up_weight, "fs", axis=0, tiled=True),

time: 514 us -> 467 us (0.909)
  waiting for transfers between devices: 439 us -> 381 us
  starting transfers between devices: 0.27 us -> 6.58 us
    all_to_all x0 -> x1, waiting for transfers between devices: none -> 59.3 us  [lay_the_things(): part_now = lax.all_to_all(z1, 'tp', 0, 0)]
    all_gather x1 -> x0, waiting for transfers between devices: 48.5 us -> none  [body(): lax.all_gather(tokens, 'tp', axis=0, tiled=True)]
    all_gather x1, waiting for transfers between devices: 43.5 us -> 0.01 us  [body(): lax.all_gather(up_weight, 'fs', axis=0, tiled=True)]
    all_gather x1, waiting for transfers between devices: 35.3 us -> 11.7 us  [body(): down_full = lax.all_gather(down_weight, 'fs', axis=1, tiled=True)]
    all_to_all x0 -> x1, starting transfers between devices: none -> 6.35 us  [lay_the_things(): part_now = lax.all_to_all(z1, 'tp', 0, 0)]
  transfers between devices with their start and end apart: 7 -> 7, of which waited for: 7 -> 6; matrix products, arithmetic and copies ran while one was open for 7% -> 9% of each run, Pallas kernels for 0% -> 0%
where the time goes in v1:
time: 467 us
  waiting for transfers between devices  381 us (82%)
  matrix products  47.4 us (10%)
  between operations  14.3 us (3%)
  local copies, waits for them, and re-layouts  9.28 us (2%)
  other arithmetic  8.62 us (2%)
  starting transfers between devices  6.58 us (1%)
    reduce_scatter x1, waiting for transfers between devices, body(): lax.psum_scatter(jnp.concatenate([over_rows(tok_all, d_gate), over_rows(t...  157 us
    reduce_scatter x1, waiting for transfers between devices, body(): lax.psum_scatter(over_cols(d_gate, gate_full) + over_cols(d_up, up_full),...  67.2 us
    all_to_all x1, waiting for transfers between devices, lay_the_things(): part_now = lax.all_to_all(z1, 'tp', 0, 0)  59.3 us
    all_gather x1, waiting for transfers between devices, body(): lax.all_gather(grad_out, 'tp', axis=0, tiled=True)  48.4 us
    all_gather x1, waiting for transfers between devices, body(): lax.all_gather(gate_weight, 'fs', axis=0, tiled=True)  34.2 us
    dot_general x3, matrix products, over_cols(): lax.dot_general(left, right, (((1,), (1,)), ((), ())), preferred_element_...  18.3 us
    dot_general x3, matrix products, over_rows(): lax.dot_general(left, right, (((0,), (0,)), ((), ())), preferred_element_...  13.2 us
    all_gather x1, waiting for transfers between devices, body(): down_full = lax.all_gather(down_weight, 'fs', axis=1, tiled=True)  11.7 us
  transfers between devices with their start and end apart: 7, of which 6 were waited for; matrix products, arithmetic and copies ran while one was open for 9% of the time, Pallas kernels for 0%

profile of v1, /device:TPU:0, one launch (start us, length us, event | category | flops | bytes accessed | tf_op | source)
XLA Modules:
  0.0 466.8 jit_solution(4492660788380723478)
XLA Ops:
  7.2 0.7 all-gather.11.cloned.1.call-update
  7.9 0.7 all-gather.9.cloned.1.call-update
  8.7 0.7 all-gather.7.cloned.1.call-update
  9.4 3.6 stack.2
  12.9 6.4 %all-to-all-start = ((bf16[8,128,2048]{2,1,0:T(8,128)(2,1)}), bf16[8,128,2048]{2,1,0:T(8,128)(2,1)}, u32[]{:S(2)}, u32[]{:S(2)}) async-start(bf16[8,128,2048]{2,1,0:T(8,128)(2,1)} %stack.2), calls=%async_computation | async-start | bytes 8388608 | tf_op jit(solution)/shard_map/all_to_all | solution.py:24
  19.3 0.5 all-gather.5.cloned.1.call-update
  19.9 34.2 %all-gather.11.cloned.1.call-done = bf16[2048,704]{0,1:T(8,128)(2,1)} async-done(((bf16[512,704]{0,1:T(8,128)(2,1)}), bf16[2048,704]{0,1:T(8,128)(2,1)}) %all-gather.11.cloned.1.call-update) | async-done | bytes 2883600 | tf_op jit(solution)/shard_map/all_gather | solution.py:29
  54.1 59.3 %all-to-all-done = bf16[8,128,2048]{2,1,0:T(8,128)(2,1)} async-done(((bf16[8,128,2048]{2,1,0:T(8,128)(2,1)}), bf16[8,128,2048]{2,1,0:T(8,128)(2,1)}, u32[]{:S(2)}, u32[]{:S(2)}) %all-to-all-start) | async-done | bytes 4194336 | tf_op jit(solution)/shard_map/all_to_all | solution.py:24
  113.4 7.9 %fusion.4 = f32[1024,704]{0,1:T(8,128)} fusion(bf16[1024,2048]{1,0:T(8,128)(2,1)} %bitcast, bf16[2048,704]{0,1:T(8,128)(2,1)} %all-gather.11.cloned.1.call-done), kind=kOutput, calls=%fused_computation.13 | convolution fusion | flops 2952790016 | bytes 9961472 | tf_op jit(solution)/shard_map/dot_general | solution.py:33
  121.3 8.0 %fusion.3 = f32[1024,704]{0,1:T(8,128)} fusion(bf16[1024,2048]{1,0:T(8,128)(2,1)} %bitcast, bf16[2048,704]{0,1:T(8,128)(2,1)} %all-gather.9.cloned.1.call-done), kind=kOutput, calls=%fused_computation.12 | convolution fusion | flops 2952790016 | bytes 9961472 | tf_op jit(solution)/shard_map/dot_general | solution.py:34
  129.2 11.7 %all-gather.7.cloned.1.call-done = bf16[704,2048]{1,0:T(8,128)(2,1)} async-done(((bf16[704,512]{1,0:T(8,128)(2,1)}), bf16[704,2048]{1,0:T(8,128)(2,1)}) %all-gather.7.cloned.1.call-update) | async-done | bytes 2883600 | tf_op jit(solution)/shard_map/all_gather | solution.py:32
  140.9 48.4 %all-gather.5.cloned.1.call-done = bf16[1024,2048]{1,0:T(8,128)(2,1)} async-done(((bf16[128,2048]{1,0:T(8,128)(2,1)}), bf16[1024,2048]{1,0:T(8,128)(2,1)}) %all-gather.5.cloned.1.call-update) | async-done | bytes 4194320 | tf_op jit(solution)/shard_map/all_gather | solution.py:27
  189.2 8.7 %multiply_convert_fusion.1 = (bf16[1024,704]{0,1:T(8,128)(2,1)S(1)}, bf16[1024,704]{0,1:T(8,128)(2,1)S(1)}) fusion(f32[1024,704]{0,1:T(8,128)} %fusion.4, f32[1024,704]{0,1:T(8,128)} %fusion.3, bf16[1024,2048]{1,0:T(8,128)(2,1)} %all-gather.5.cloned.1.call-done, bf16[704,2048]{1,0:T(8,128)(2,1)} %all-gather.7.cloned.1.call-done), kind=kOutput, calls=%fused_computation.6 | convolution fusion | flops 2962161664 | bytes 15728640 | tf_op jit(solution)/shard_map/dot_general | solution.py:14
  198.0 3.5 fusion.5
  201.6 6.0 %convolution_add_fusion = f32[1024,2048]{1,0:T(8,128)} fusion(f32[1024,2048]{1,0:T(8,128)S(1)} %fusion.5, bf16[1024,704]{0,1:T(8,128)(2,1)S(1)} %get-tuple-element.4, bf16[2048,704]{0,1:T(8,128)(2,1)S(1)} %copy-done.2), kind=kOutput, calls=%fused_computation.1 | convolution fusion | flops 2954887168 | bytes 21102592 | tf_op jit(solution)/shard_map/dot_general | solution.py:14
  207.7 1.3 copy-done.4
  209.0 4.9 %convolution_bitcast_fusion.1 = f32[2048,704]{0,1:T(8,128)S(1)} fusion(bf16[1024,704]{0,1:T(8,128)(2,1)S(1)} %copy-done.4, bf16[1024,2048]{1,0:T(8,128)(2,1)} %bitcast), kind=kOutput, calls=%fused_computation.3 | convolution fusion | flops 2952790016 | bytes 11403264 | tf_op jit(solution)/shard_map/dot_general | solution.py:8
  214.0 5.1 %convolution_bitcast_fusion.2 = f32[2048,704]{0,1:T(8,128)S(1)} fusion(bf16[1024,704]{0,1:T(8,128)(2,1)S(1)} %copy-done.6, bf16[1024,2048]{1,0:T(8,128)(2,1)} %bitcast), kind=kOutput, calls=%fused_computation.4 | convolution fusion | flops 2952790016 | bytes 11403264 | tf_op jit(solution)/shard_map/dot_general | solution.py:8
  219.1 3.2 convolution_bitcast_fusion
  222.3 6.5 %pad_maximum_fusion = f32[2048,2112]{0,1:T(8,128)} fusion(f32[2048,704]{0,1:T(8,128)S(1)} %convolution_bitcast_fusion, f32[2048,704]{0,1:T(8,128)S(1)} %convolution_bitcast_fusion.1, f32[2048,704]{0,1:T(8,128)S(1)} %convolution_bitcast_fusion.2), kind=kLoop, calls=%fused_computation | loop fusion | flops 8650752 | bytes 34603008 | tf_op jit(solution)/shard_map/concatenate | solution.py:51
  228.9 67.2 %reduce-scatter.3.cloned.1.call-done = f32[128,2048]{1,0:T(8,128)} async-done(((f32[1024,2048]{1,0:T(8,128)}), f32[128,2048]{1,0:T(8,128)}) %reduce-scatter.3.cloned.1.call-update) | async-done | bytes 1048592 | tf_op jit(solution)/shard_map/reduce_scatter | solution.py:43
  296.2 2.1 convert_element_type.14
  298.2 157.4 %reduce-scatter.5.cloned.1.call-done = f32[512,2112]{0,1:T(8,128)} async-done(((f32[2048,2112]{0,1:T(8,128)}), f32[512,2112]{0,1:T(8,128)}) %reduce-scatter.5.cloned.1.call-update) | async-done | bytes 4325392 | tf_op jit(solution)/shard_map/reduce_scatter | solution.py:50
  455.6 4.4 slice_bitcast_fusion
  (26 shorter events, 0.3 us)
Async XLA Ops:
  7.2 46.9 %all-gather.11.cloned.1.call-start = ((), (), s32[]{:S(2)}) async-start(), calls=%async_computation.6 | async-start | bytes 3604480 | tf_op jit(solution)/shard_map/all_gather | solution.py:29
  7.9 113.4 %all-gather.9.cloned.1.call-start = ((), (), s32[]{:S(2)}) async-start(), calls=%async_computation.5 | async-start | bytes 3604480 | tf_op jit(solution)/shard_map/all_gather | solution.py:30
  8.6 132.2 %all-gather.7.cloned.1.call-start = ((), (), s32[]{:S(2)}) async-start(), calls=%async_computation.4 | async-start | bytes 3604480 | tf_op jit(solution)/shard_map/all_gather | solution.py:32
  12.9 100.4 %all-to-all-start = ((bf16[8,128,2048]{2,1,0:T(8,128)(2,1)}), bf16[8,128,2048]{2,1,0:T(8,128)(2,1)}, u32[]{:S(2)}, u32[]{:S(2)}) async-start(bf16[8,128,2048]{2,1,0:T(8,128)(2,1)} %stack.2), calls=%async_computation | async-start | bytes 8388608 | tf_op jit(solution)/shard_map/all_to_all | solution.py:24
  19.3 170.0 %all-gather.5.cloned.1.call-start = ((), (), s32[]{:S(2)}) async-start(), calls=%async_computation.3 | async-start | bytes 4718592 | tf_op jit(solution)/shard_map/all_gather | solution.py:27
  19.9 276.3 %reduce-scatter.3.cloned.1.call-start = ((), (), s32[]{:S(2)}) async-start(), calls=%async_computation.7 | async-start | bytes 9437184 | tf_op jit(solution)/shard_map/reduce_scatter | solution.py:43
  129.2 68.8 %copy-start.1 = (bf16[2048,704]{0,1:T(8,128)(2,1)S(1)}, bf16[2048,704]{0,1:T(8,128)(2,1)}, u32[]{:S(2)}) copy-start(bf16[2048,704]{0,1:T(8,128)(2,1)} %all-gather.11.cloned.1.call-done) | copy-start | bytes 8650756
  198.0 3.6 copy-start.5
  198.0 3.6 copy-start.3
  198.0 3.6 copy-start.2
  207.6 1.4 copy-start.4
  207.7 6.3 %copy-start.6 = (bf16[1024,704]{0,1:T(8,128)(2,1)S(1)}, bf16[1024,704]{0,1:T(8,128)(2,1)}, u32[]{:S(2)}) copy-start(bf16[1024,704]{0,1:T(8,128)(2,1)} %copy-done.5) | copy-start | bytes 4325380
  207.7 247.9 %reduce-scatter.5.cloned.1.call-start = ((), (), s32[]{:S(2)}) async-start(), calls=%async_computation.8 | async-start | bytes 21626880 | tf_op jit(solution)/shard_map/reduce_scatter | solution.py:50
  213.9 5.1 %copy-start = (bf16[1024,2048]{1,0:T(8,128)(2,1)S(1)}, bf16[1024,2048]{1,0:T(8,128)(2,1)}, u32[]{:S(2)}) copy-start(bf16[1024,2048]{1,0:T(8,128)(2,1)} %all-gather.5.cloned.1.call-done) | copy-start | bytes 12582916
  214.0 5.1 %copy-start.7 = (f32[1024,704]{0,1:T(8,128)S(1)}, f32[1024,704]{0,1:T(8,128)}, u32[]{:S(2)}) copy-start(f32[1024,704]{0,1:T(8,128)} %fusion.4) | copy-start | bytes 8650756
  214.0 5.2 %copy-start.8 = (f32[1024,704]{0,1:T(8,128)S(1)}, f32[1024,704]{0,1:T(8,128)}, u32[]{:S(2)}) copy-start(f32[1024,704]{0,1:T(8,128)} %fusion.3) | copy-start | bytes 8650756
Sparse Core Ops, SparseCore 0:
  9.8 44.2 all-gather.10
  55.9 41.5 all-gather.8
  99.3 41.5 all-gather.6
  142.4 46.8 all-gather.4
  207.8 88.3 reduce-scatter.2
  299.1 156.4 reduce-scatter.4
